TPU v7x, 32 devices: a whole 2x2x4 slice. The times are simulated.
32 devices in a mesh: sp: 4 (over z), dp: 8 (over y, x, core).
Axes of the slice: x: 2, y: 2, z: 4, core: 2. Of those that a mesh axis runs over, the one named last changes fastest.
Arguments:
- tokens: bfloat16 [8, 256, 2048], P('dp', 'sp'), may hold values from -6 to 6
- query_weight: bfloat16 [2048, 512], P('dp'), may hold values from -0.125 to 0.125
- key_weight: bfloat16 [2048, 512], P('dp'), may hold values from -0.125 to 0.125
- value_weight: bfloat16 [2048, 1024], P('dp'), may hold values from -0.125 to 0.125
- gate_weight: bfloat16 [2048, 4, 16], P('dp'), may hold values from -0.125 to 0.125
- gate_bias: float32 [4, 16], P(None, 'sp'), may hold values from 2 to 6
- norm_gain: float32 [16, 64], P('sp'), may hold values from 0.5 to 1.5
- out_weight: bfloat16 [1024, 2048], P(None, 'dp'), may hold values from -0.1875 to 0.1875
Outputs:
- mixed: bfloat16 [8, 256, 2048], P('dp', 'sp')
All inputs are finite; a program needn't handle non-finite values.
Results may differ from a plain program's by a relative error of at most 0.005.
Values may be sent and summed in bfloat16 or wider, within the bound.
A program may use at most 64 MiB of HBM per device.

v0:
```python
import jax
import jax.numpy as jnp
from jax import lax
from jax.sharding import PartitionSpec as P

BLOCK = 64


norm_eps = 1e-06


def block_scan(queries, key_rows, value_rows, input_gate, log_forget):
    length = queries.shape[0]
    block_count = length // BLOCK
    key_width = queries.shape[1]
    value_width = value_rows.shape[1]
    high = lax.Precision.HIGHEST

    def reshape_blocks(array):
        return array.reshape((block_count, BLOCK) + array.shape[1:])

    causal_mask = jnp.tril(jnp.ones((BLOCK, BLOCK), dtype=bool))

    def advance(carried_state, pieces):
        memory, normal, stabilizer = carried_state
        query_block, key_block, value_block, input_block, forget_block = pieces
        forget_sum = jnp.cumsum(forget_block)
        log_weights = forget_sum[:, None] - forget_sum[None, :] + input_block[None, :]
        log_weights = jnp.where(causal_mask, log_weights, -jnp.inf)
        carry_log = forget_sum + stabilizer
        stab_row = jnp.maximum(carry_log, jnp.max(log_weights, axis=1))
        scores = jnp.dot(query_block, key_block.T, precision=high) * jnp.exp(
            log_weights - stab_row[:, None]
        )
        carried = jnp.exp(carry_log - stab_row)
        numerator = carried[:, None] * jnp.dot(query_block, memory, precision=high) + jnp.dot(
            scores, value_block, precision=high
        )
        denominator = carried * jnp.dot(query_block, normal, precision=high) + jnp.sum(
            scores, axis=1
        )
        hidden = numerator / jnp.maximum(jnp.abs(denominator), jnp.exp(-stab_row))[:, None]
        forget_total = forget_sum[-1]
        weights_in = forget_total - forget_sum + input_block
        new_stabilizer = jnp.maximum(forget_total + stabilizer, jnp.max(weights_in))
        decay_old = jnp.exp(forget_total + stabilizer - new_stabilizer)
        weights_in = jnp.exp(weights_in - new_stabilizer)
        memory = decay_old * memory + jnp.dot(
            (key_block * weights_in[:, None]).T, value_block, precision=high
        )
        normal = decay_old * normal + jnp.dot(weights_in, key_block, precision=high)
        return ((memory, normal, new_stabilizer), hidden)

    init_state = (
        jnp.zeros((key_width, value_width), jnp.float32),
        jnp.zeros((key_width,), jnp.float32),
        jnp.zeros((), jnp.float32),
    )
    pieces = (
        reshape_blocks(queries),
        reshape_blocks(key_rows),
        reshape_blocks(value_rows),
        reshape_blocks(input_gate),
        reshape_blocks(log_forget),
    )
    final_state, outputs = lax.scan(advance, init_state, pieces)
    return outputs.reshape(length, value_width)


def reverse_time(array):
    return jnp.flip(array, axis=2)


def mix_heads(queries, keys_in, values_in, gate_pre, norm_gain):
    scale_factor = queries.shape[-1] ** (-0.5)
    query_major = jnp.transpose(queries.astype(jnp.float32), (0, 2, 1, 3)) * scale_factor
    key_major = jnp.transpose(keys_in.astype(jnp.float32), (0, 2, 1, 3))
    value_major = jnp.transpose(values_in.astype(jnp.float32), (0, 2, 1, 3))
    gate_major = jnp.transpose(gate_pre, (2, 0, 3, 1))
    input_forward = gate_major[0]
    forget_forward = jax.nn.log_sigmoid(gate_major[1])
    input_backward = gate_major[2]
    forget_backward = jax.nn.log_sigmoid(gate_major[3])
    scan_all = jax.vmap(jax.vmap(block_scan))
    forward = scan_all(query_major, key_major, value_major, input_forward, forget_forward)
    backward = reverse_time(
        scan_all(
            reverse_time(query_major),
            reverse_time(key_major),
            reverse_time(value_major),
            reverse_time(input_backward),
            reverse_time(forget_backward),
        )
    )
    combined = forward + backward
    normed = combined * lax.rsqrt(jnp.mean(combined * combined, axis=-1, keepdims=True) + norm_eps)
    normed = normed * norm_gain[None, :, None, :]
    return jnp.transpose(normed, (0, 2, 1, 3)).astype(jnp.bfloat16)


def add_product(partial_value, flat_tokens, weight_rows, offset):
    row_count = weight_rows.shape[0]
    columns = lax.dynamic_slice_in_dim(flat_tokens, offset, row_count, 1)
    return partial_value + jnp.dot(
        columns, weight_rows.reshape(row_count, -1), preferred_element_type=jnp.float32
    )


def local(
    tokens, query_weight, key_weight, value_weight, gate_weight, gate_bias, norm_gain, out_weight
):
    batch_local, token_count, model_width = tokens.shape
    flat_tokens = tokens.reshape(batch_local * token_count, model_width)
    row_total = flat_tokens.shape[0]
    head_count = gate_weight.shape[2]
    key_width = query_weight.shape[1] // head_count
    value_width = value_weight.shape[1] // head_count
    empty_query = jnp.zeros((row_total, query_weight.shape[1]), jnp.float32)
    empty_value = jnp.zeros((row_total, value_weight.shape[1]), jnp.float32)
    empty_gate = jnp.zeros((row_total, 4 * head_count), jnp.float32)

    def fold_one(partial_value, weight_rows, offset):
        return add_product(partial_value, flat_tokens, weight_rows, offset)

    query_raw = fold_one(
        empty_query,
        jax.tree.map(lambda part: lax.all_gather(part, "dp", axis=0, tiled=True), query_weight),
        jnp.int32(0),
    )
    key_raw = fold_one(
        empty_query,
        jax.tree.map(lambda part: lax.all_gather(part, "dp", axis=0, tiled=True), key_weight),
        jnp.int32(0),
    )
    value_raw = fold_one(
        empty_value,
        jax.tree.map(lambda part: lax.all_gather(part, "dp", axis=0, tiled=True), value_weight),
        jnp.int32(0),
    )
    gate_raw = fold_one(
        empty_gate,
        jax.tree.map(lambda part: lax.all_gather(part, "dp", axis=0, tiled=True), gate_weight),
        jnp.int32(0),
    )
    query_local = query_raw.astype(jnp.bfloat16).reshape(
        batch_local, token_count, head_count, key_width
    )
    key_local = key_raw.astype(jnp.bfloat16).reshape(
        batch_local, token_count, head_count, key_width
    )
    value_local = value_raw.astype(jnp.bfloat16).reshape(
        batch_local, token_count, head_count, value_width
    )
    query_local, key_local, value_local = (
        lax.all_to_all(query_local, "sp", split_axis=2, concat_axis=1, tiled=True),
        lax.all_to_all(key_local, "sp", split_axis=2, concat_axis=1, tiled=True),
        lax.all_to_all(value_local, "sp", split_axis=2, concat_axis=1, tiled=True),
    )
    gate_local = gate_raw.reshape(batch_local, token_count, 4, head_count)
    gate_local = (
        lax.all_to_all(gate_local, "sp", split_axis=3, concat_axis=1, tiled=True)
        + gate_bias[None, None]
    )
    normed = mix_heads(query_local, key_local, value_local, gate_local, norm_gain)
    returned = lax.all_to_all(normed, "sp", split_axis=1, concat_axis=2, tiled=True)
    hidden_flat = returned.reshape(row_total, -1)

    def project(weight_cols):
        return jnp.dot(hidden_flat, weight_cols, preferred_element_type=jnp.float32)

    output = project(lax.all_gather(out_weight, "dp", axis=1, tiled=True))
    return output.astype(jnp.bfloat16).reshape(batch_local, token_count, model_width)


def solution(mesh):
    return jax.shard_map(
        local,
        mesh=mesh,
        in_specs=(
            P("dp", "sp", None),
            P("dp", None),
            P("dp", None),
            P("dp", None),
            P("dp", None, None),
            P(None, "sp"),
            P("sp", None),
            P(None, "dp"),
        ),
        out_specs=P("dp", "sp", None),
        check_vma=False,
    )
```

profile of v0, /device:TPU:0, one launch (start us, length us, event | category | flops | bytes accessed | tf_op | source)
XLA Modules:
  0.0 174.4 jit_solution(13415725954093532424)
XLA Ops:
  6.5 0.7 all-gather.5.cloned.1.call-update
  7.3 0.7 all-gather.9.cloned.1.call-update
  8.1 0.7 all-gather.7.cloned.1.call-update
  8.7 11.6 %all_gather.15 = bf16[2048,4,16]{0,2,1:T(8,128)(2,1)S(1)} all-gather(bf16[256,4,16]{0,2,1:T(8,128)(2,1)} %param.16), channel_id=1, replica_groups=mesh['sp'=4,'dp'=8] {'dp'}, dimensions={0}, use_global_device_ids=true | all-gather | bytes 294912 | tf_op jit(solution)/shard_map/all_gather | solution.py:142
  20.6 0.7 reshape.803
  21.3 4.9 %all-to-all-start = ((f32[4,1,1024]{2,1,0:T(1,128)}), f32[4,1,1024]{2,1,0:T(1,128)S(1)}, u32[]{:S(2)}, u32[]{:S(2)}) async-start(f32[4,1,1024]{2,1,0:T(1,128)} %reshape.803), calls=%async_computation | async-start | bytes 32768 | tf_op jit(solution)/shard_map/all_to_all | solution.py:161
  26.1 0.6 all-gather.11.cloned.1.call-update
  26.8 5.0 %all-to-all-done = f32[4,1,1024]{2,1,0:T(1,128)S(1)} async-done(((f32[4,1,1024]{2,1,0:T(1,128)}), f32[4,1,1024]{2,1,0:T(1,128)S(1)}, u32[]{:S(2)}, u32[]{:S(2)}) %all-to-all-start) | async-done | bytes 16416 | tf_op jit(solution)/shard_map/all_to_all | solution.py:161
  31.8 0.5 broadcast.372
  32.3 0.7 reduce.15
  33.2 0.8 add_bitcast_fusion
  34.0 5.5 %all-gather.5.cloned.1.call-done = bf16[2048,512]{1,0:T(8,128)(2,1)} async-done(((bf16[256,512]{1,0:T(8,128)(2,1)}), bf16[2048,512]{1,0:T(8,128)(2,1)}) %all-gather.5.cloned.1.call-update) | async-done | bytes 2097168 | tf_op jit(solution)/shard_map/all_gather | solution.py:132
  39.6 2.1 %convolution_convert_fusion.3 = bf16[64,512]{1,0:T(8,128)(2,1)S(1)} fusion(bf16[2048,512]{1,0:T(8,128)(2,1)} %all-gather.5.cloned.1.call-done, bf16[1,64,2048]{2,1,0:T(8,128)(2,1)S(1)} %copy-done), kind=kOutput, calls=%fused_computation.76 | convolution fusion | flops 134250496 | bytes 2424832 | tf_op jit(solution)/shard_map/dot_general | solution.py:104
  41.8 0.8 reshape.805
  42.6 4.6 %all-to-all-start.1 = ((bf16[4,2,4096]{2,1,0:T(2,128)(2,1)}), bf16[4,2,4096]{2,1,0:T(2,128)(2,1)S(1)}, u32[]{:S(2)}, u32[]{:S(2)}) async-start(bf16[4,2,4096]{2,1,0:T(2,128)(2,1)} %reshape.805), calls=%async_computation.1 | async-start | bytes 131072 | tf_op jit(solution)/shard_map/all_to_all | solution.py:156
  47.2 21.9 %all-gather.9.cloned.1.call-done = bf16[2048,512]{1,0:T(8,128)(2,1)} async-done(((bf16[256,512]{1,0:T(8,128)(2,1)}), bf16[2048,512]{1,0:T(8,128)(2,1)}) %all-gather.9.cloned.1.call-update) | async-done | bytes 2097168 | tf_op jit(solution)/shard_map/all_gather | solution.py:127
  69.1 2.1 %convolution_convert_fusion.2 = bf16[64,512]{1,0:T(8,128)(2,1)S(1)} fusion(bf16[2048,512]{1,0:T(8,128)(2,1)} %all-gather.9.cloned.1.call-done, bf16[1,64,2048]{2,1,0:T(8,128)(2,1)S(1)} %copy-done), kind=kOutput, calls=%fused_computation.75 | convolution fusion | flops 134250496 | bytes 2424832 | tf_op jit(solution)/shard_map/dot_general | solution.py:104
  71.3 0.8 reshape.809
  72.1 4.6 %all-to-all-start.3 = ((bf16[4,2,4096]{2,1,0:T(2,128)(2,1)}), bf16[4,2,4096]{2,1,0:T(2,128)(2,1)S(1)}, u32[]{:S(2)}, u32[]{:S(2)}) async-start(bf16[4,2,4096]{2,1,0:T(2,128)(2,1)} %reshape.809), calls=%async_computation.3 | async-start | bytes 131072 | tf_op jit(solution)/shard_map/all_to_all | solution.py:155
  78.1 4.3 %all-to-all-done.3 = bf16[4,2,4096]{2,1,0:T(2,128)(2,1)S(1)} async-done(((bf16[4,2,4096]{2,1,0:T(2,128)(2,1)}), bf16[4,2,4096]{2,1,0:T(2,128)(2,1)S(1)}, u32[]{:S(2)}, u32[]{:S(2)}) %all-to-all-start.3) | async-done | bytes 65568 | tf_op jit(solution)/shard_map/all_to_all | solution.py:155
  83.3 24.1 %all-gather.7.cloned.1.call-done = bf16[2048,1024]{1,0:T(8,128)(2,1)} async-done(((bf16[256,1024]{1,0:T(8,128)(2,1)}), bf16[2048,1024]{1,0:T(8,128)(2,1)}) %all-gather.7.cloned.1.call-update) | async-done | bytes 4194320 | tf_op jit(solution)/shard_map/all_gather | solution.py:137
  107.4 3.0 %convolution_convert_fusion.1 = bf16[64,1024]{1,0:T(8,128)(2,1)S(1)} fusion(bf16[2048,1024]{1,0:T(8,128)(2,1)} %all-gather.7.cloned.1.call-done, bf16[1,64,2048]{2,1,0:T(8,128)(2,1)S(1)} %copy-done), kind=kOutput, calls=%fused_computation.74 | convolution fusion | flops 268500992 | bytes 4587520 | tf_op jit(solution)/shard_map/dot_general | solution.py:104
  110.7 0.9 reshape.807
  111.6 4.6 %all-to-all-start.2 = ((bf16[4,2,8192]{2,1,0:T(2,128)(2,1)}), bf16[4,2,8192]{2,1,0:T(2,128)(2,1)S(1)}, u32[]{:S(2)}, u32[]{:S(2)}) async-start(bf16[4,2,8192]{2,1,0:T(2,128)(2,1)} %reshape.807), calls=%async_computation.2 | async-start | bytes 262144 | tf_op jit(solution)/shard_map/all_to_all | solution.py:157
  116.5 6.5 %all-to-all-done.2 = bf16[4,2,8192]{2,1,0:T(2,128)(2,1)S(1)} async-done(((bf16[4,2,8192]{2,1,0:T(2,128)(2,1)}), bf16[4,2,8192]{2,1,0:T(2,128)(2,1)S(1)}, u32[]{:S(2)}, u32[]{:S(2)}) %all-to-all-start.2) | async-done | bytes 131104 | tf_op jit(solution)/shard_map/all_to_all | solution.py:157
  124.5 13.9 %while.36 = (s32[]{:T(128)}, f32[1,4,32,64]{3,2,1,0:T(8,128)S(1)}, f32[1,4,32]{2,1,0:T(4,128)S(1)}, f32[1,4]{1,0:T(1,128)S(1)}, f32[4,1,4,64,64]{4,3,2,1,0:T(8,1...) while((s32[]{:T(128)}, f32[1,4,32,64]{3,2,1,0:T(8,128)S(1)}, ...), condition=%wide.region_5.6_spmd.clone.clone, body=%wide.region_0.5_spmd.clone.clone.sunk | while | flops 31931792 | bytes 1270174 | solution.py:66
  126.1 0.4 fusion.124
  133.1 0.4 fusion.124
  139.2 13.8 %while.37 = (s32[]{:T(128)}, f32[1,4,32,64]{3,2,1,0:T(8,128)S(1)}, f32[1,4,32]{2,1,0:T(4,128)S(1)}, f32[1,4]{1,0:T(1,128)S(1)}, f32[4,1,4,64,64]{4,3,2,1,0:T(8,1...) while((s32[]{:T(128)}, f32[1,4,32,64]{3,2,1,0:T(8,128)S(1)}, ...), condition=%wide.region_11.12_spmd.clone.clone, body=%wide.region_6.11_spmd.clone.clone.sunk | while | flops 31931792 | bytes 1270174 | solution.py:66
  140.9 0.4 fusion.142
  154.5 9.0 %all_to_all.60 = bf16[4,2,8192]{2,1,0:T(2,128)(2,1)S(1)} all-to-all(bf16[4,2,8192]{2,1,0:T(2,128)(2,1)S(1)} %reshape.811), channel_id=1, replica_groups=mesh['sp'=4,'dp'=8] {'sp'}, dimensions={0} | all-to-all | bytes 262144 | tf_op jit(solution)/shard_map/all_to_all | solution.py:165
  164.1 3.7 %fusion.30 = bf16[1,64,2048]{2,1,0:T(8,128)(2,1)} fusion(bf16[64,1024]{1,0:T(8,128)(2,1)S(1)} %reshape.766, bf16[1024,2048]{1,0:T(8,128)(2,1)} %all-gather.11.cloned.1.call-done), kind=kOutput, calls=%fused_computation.73 | convolution fusion | flops 268566528 | bytes 4587520 | tf_op jit(solution)/shard_map/dot_general | solution.py:169
  (219 shorter events, 33.6 us)
Async XLA Ops:
  6.5 13.8 %copy-start = (bf16[1,64,2048]{2,1,0:T(8,128)(2,1)S(1)}, bf16[1,64,2048]{2,1,0:T(8,128)(2,1)}, u32[]{:S(2)}) copy-start(bf16[1,64,2048]{2,1,0:T(8,128)(2,1)} %param.12) | copy-start | bytes 786436
  6.5 33.0 %all-gather.5.cloned.1.call-start = ((), (), s32[]{:S(2)}) async-start(), calls=%async_computation.5 | async-start | bytes 2359296 | tf_op jit(solution)/shard_map/all_gather | solution.py:132
  7.3 61.8 %all-gather.9.cloned.1.call-start = ((), (), s32[]{:S(2)}) async-start(), calls=%async_computation.7 | async-start | bytes 2359296 | tf_op jit(solution)/shard_map/all_gather | solution.py:127
  8.0 99.4 %all-gather.7.cloned.1.call-start = ((), (), s32[]{:S(2)}) async-start(), calls=%async_computation.6 | async-start | bytes 4718592 | tf_op jit(solution)/shard_map/all_gather | solution.py:137
  21.3 10.5 %all-to-all-start = ((f32[4,1,1024]{2,1,0:T(1,128)}), f32[4,1,1024]{2,1,0:T(1,128)S(1)}, u32[]{:S(2)}, u32[]{:S(2)}) async-start(f32[4,1,1024]{2,1,0:T(1,128)} %reshape.803), calls=%async_computation | async-start | bytes 32768 | tf_op jit(solution)/shard_map/all_to_all | solution.py:161
  26.1 138.0 %all-gather.11.cloned.1.call-start = ((), (), s32[]{:S(2)}) async-start(), calls=%async_computation.8 | async-start | bytes 4718592 | tf_op jit(solution)/shard_map/all_gather | solution.py:171
  42.6 29.5 %all-to-all-start.1 = ((bf16[4,2,4096]{2,1,0:T(2,128)(2,1)}), bf16[4,2,4096]{2,1,0:T(2,128)(2,1)S(1)}, u32[]{:S(2)}, u32[]{:S(2)}) async-start(bf16[4,2,4096]{2,1,0:T(2,128)(2,1)} %reshape.805), calls=%async_computation.1 | async-start | bytes 131072 | tf_op jit(solution)/shard_map/all_to_all | solution.py:156
  72.1 10.3 %all-to-all-start.3 = ((bf16[4,2,4096]{2,1,0:T(2,128)(2,1)}), bf16[4,2,4096]{2,1,0:T(2,128)(2,1)S(1)}, u32[]{:S(2)}, u32[]{:S(2)}) async-start(bf16[4,2,4096]{2,1,0:T(2,128)(2,1)} %reshape.809), calls=%async_computation.3 | async-start | bytes 131072 | tf_op jit(solution)/shard_map/all_to_all | solution.py:155
  111.6 11.5 %all-to-all-start.2 = ((bf16[4,2,8192]{2,1,0:T(2,128)(2,1)}), bf16[4,2,8192]{2,1,0:T(2,128)(2,1)S(1)}, u32[]{:S(2)}, u32[]{:S(2)}) async-start(bf16[4,2,8192]{2,1,0:T(2,128)(2,1)} %reshape.807), calls=%async_computation.2 | async-start | bytes 262144 | tf_op jit(solution)/shard_map/all_to_all | solution.py:157
  139.2 14.8 %copy-start.1 = (f32[4,64]{1,0:T(4,128)S(1)}, f32[4,64]{1,0:T(4,128)}, u32[]{:S(2)}) copy-start(f32[4,64]{1,0:T(4,128)} %param.18) | copy-start | bytes 3076
Sparse Core Ops, SparseCore 0:
  9.2 30.3 all-gather.4
  41.5 27.5 all-gather.8
  71.0 36.3 all-gather.6
  109.1 37.3 all-gather.10
where the time goes:
time: 175 us; the launch traced here: 174 us
  waiting for transfers between devices  70 us (40%)
  matrix products  26.6 us (15%)
  blocking collectives  20.6 us (12%)
  starting transfers between devices  18.8 us (11%)
  local copies, waits for them, and re-layouts  15.5 us (9%)
  between operations  13.5 us (8%)
  other arithmetic  8.71 us (5%)
    all_gather x3, waiting for transfers between devices, local(): lax.all_gather(part, 'dp', axis=0, tiled=True)  51.6 us
    all_gather x1, blocking collectives, local(): lax.all_gather(part, 'dp', axis=0, tiled=True)  11.6 us
    all_to_all x1, blocking collectives, local(): lax.all_to_all(normed, 'sp', split_axis=1, concat_axis=2, tiled=True)  9.04 us
    dot_general x4, matrix products, add_product(): jnp.dot(columns, weight_rows.reshape(row_count, -1), preferred_element_ty...  7.38 us
    all_to_all x1, waiting for transfers between devices, local(): lax.all_to_all(value_local, 'sp', split_axis=2, concat_axis=1, tiled=True)  6.53 us
    all_to_all x1, waiting for transfers between devices, local(): lax.all_to_all(gate_local, 'sp', split_axis=3, concat_axis=1, tiled=True)  4.99 us
    all_to_all x1, starting transfers between devices, local(): lax.all_to_all(gate_local, 'sp', split_axis=3, concat_axis=1, tiled=True)  4.87 us
    all_to_all x1, starting transfers between devices, local(): lax.all_to_all(key_local, 'sp', split_axis=2, concat_axis=1, tiled=True)  4.63 us
  transfers between devices with their start and end apart: 8, of which 6 were waited for; matrix products, arithmetic and copies ran while one was open for 27% of the time, Pallas kernels for 0%

commit v1 on v0

--- a/solution.py
+++ b/solution.py
@@ -1,6 +1,10 @@
+import functools
+
 import jax
 import jax.numpy as jnp
 from jax import lax
+from jax.experimental import pallas as pl
+from jax.experimental.pallas import tpu as pltpu
 from jax.sharding import PartitionSpec as P
 
 BLOCK = 64
@@ -172,9 +176,449 @@
     return output.astype(jnp.bfloat16).reshape(batch_local, token_count, model_width)
 
 
+MESH = pl.DeviceIdType.MESH
+PARTS = 2
+
+
+def scan_rows(values, combine, identity, backward):
+    rows = values.shape[0]
+    row_index = lax.broadcasted_iota(jnp.int32, values.shape, 0)
+    step = 1
+    while step < rows:
+        if backward:
+            moved = pltpu.roll(values, rows - step, 0)
+            moved = jnp.where(row_index < rows - step, moved, identity)
+        else:
+            moved = pltpu.roll(values, step, 0)
+            moved = jnp.where(row_index >= step, moved, identity)
+        values = combine(values, moved)
+        step *= 2
+    return values
+
+
+def fused_kernel(
+    sp,
+    head_count,
+    tokens_ref,
+    query_ref,
+    key_ref,
+    value_ref,
+    gate_ref,
+    out_weight_ref,
+    bias_ref,
+    gain_ref,
+    out_ref,
+    tok,
+    wide,
+    gates,
+    outw,
+    normed_buf,
+    hidden,
+    local_sem,
+    tok_send,
+    tok_recv,
+    wide_send,
+    wide_recv,
+    gate_send,
+    gate_recv,
+    outw_send,
+    outw_recv,
+    norm_send,
+    norm_recv,
+):
+    s = lax.axis_index("sp")
+    d = lax.axis_index("dp")
+    core = d % 2
+    xpos = (d // 2) % 2
+    ypos = d // 4
+    mate = d + 1 - 2 * core
+    xn = d + 2 - 4 * xpos
+    yn = d + 4 - 8 * ypos
+    diag = xn + 4 - 8 * ypos
+    relay_from = yn + core * (xn - yn)
+    relay_to = xn + core * (yn - xn)
+    hop = mate - d
+
+    slab = query_ref.shape[0]
+    key_cols = query_ref.shape[1] // sp
+    value_cols = value_ref.shape[1] // sp
+    gate_rows = gate_ref.shape[0]
+    block = tokens_ref.shape[0]
+    inner = out_weight_ref.shape[0]
+    piece = inner // PARTS
+    local_heads = head_count // sp
+    key_width = key_cols // local_heads
+    value_width = value_cols // local_heads
+    rows = sp * block
+
+    def wide_slot(index):
+        return wide.at[pl.ds(pl.multiple_of(index * slab, slab), slab), :]
+
+    def gate_slot(index):
+        return gates.at[pl.ds(pl.multiple_of(index * gate_rows, gate_rows), gate_rows), :]
+
+    def outw_slot(index, part):
+        return outw.at[index, pl.ds(part * piece, piece), :]
+
+    def push(ref, send, recv, axis, target):
+        return pltpu.make_async_remote_copy(
+            src_ref=ref,
+            dst_ref=ref,
+            send_sem=send,
+            recv_sem=recv,
+            device_id={axis: target},
+            device_id_type=MESH,
+        )
+
+    def wide_push(index, number, target):
+        return push(wide_slot(index), wide_send.at[number], wide_recv.at[index], "dp", target)
+
+    def gate_push(index, number, target):
+        return push(gate_slot(index), gate_send.at[number], gate_recv.at[index], "dp", target)
+
+    def outw_push(index, part, number, target):
+        return push(
+            outw_slot(index, part),
+            outw_send.at[number, part],
+            outw_recv.at[index, part],
+            "dp",
+            target,
+        )
+
+    def tok_push(origin, number, target):
+        return push(tok.at[origin], tok_send.at[number], tok_recv.at[origin], "sp", target)
+
+    key_at = pl.multiple_of(s * key_cols, key_cols)
+    value_at = pl.multiple_of(s * value_cols, value_cols)
+    own_rows = pl.ds(pl.multiple_of(d * slab, slab), slab)
+    loads = [
+        pltpu.make_async_copy(tokens_ref, tok.at[s], local_sem.at[0]),
+        pltpu.make_async_copy(
+            query_ref.at[:, pl.ds(key_at, key_cols)],
+            wide.at[own_rows, pl.ds(0, key_cols)],
+            local_sem.at[1],
+        ),
+        pltpu.make_async_copy(
+            key_ref.at[:, pl.ds(key_at, key_cols)],
+            wide.at[own_rows, pl.ds(key_cols, key_cols)],
+            local_sem.at[2],
+        ),
+        pltpu.make_async_copy(
+            value_ref.at[:, pl.ds(value_at, value_cols)],
+            wide.at[own_rows, pl.ds(2 * key_cols, value_cols)],
+            local_sem.at[3],
+        ),
+        pltpu.make_async_copy(gate_ref, gate_slot(d), local_sem.at[4]),
+        pltpu.make_async_copy(out_weight_ref, outw.at[d], local_sem.at[5]),
+    ]
+    for load in loads:
+        load.start()
+
+    barrier = pltpu.get_barrier_semaphore()
+    for target in (xn, yn, mate):
+        pl.semaphore_signal(barrier, inc=1, device_id={"dp": target}, device_id_type=MESH)
+    for offset in range(1, sp):
+        pl.semaphore_signal(
+            barrier, inc=1, device_id={"sp": (s + offset) % sp}, device_id_type=MESH
+        )
+    pl.semaphore_wait(barrier, 3 + sp - 1)
+
+    def token_stage(k, wait):
+        right_origin = s - k
+        left_origin = s + k
+        has_left = right_origin >= 0
+        has_right = left_origin < sp
+        if wait:
+
+            @pl.when(has_left)
+            def _():
+                tok_push(right_origin, 0, s).wait_recv()
+
+        @pl.when(jnp.logical_and(has_left, s + 1 < sp))
+        def _():
+            tok_push(right_origin, 2 * k, s + 1).start()
+
+        if wait:
+
+            @pl.when(has_right)
+            def _():
+                tok_push(left_origin, 0, s).wait_recv()
+
+        @pl.when(jnp.logical_and(has_right, s >= 1))
+        def _():
+            tok_push(left_origin, 2 * k + 1, s - 1).start()
+
+    def token_drain(k):
+        @pl.when(jnp.logical_and(s - k >= 0, s + 1 < sp))
+        def _():
+            tok_push(s - k, 2 * k, s + 1).wait_send()
+
+        @pl.when(jnp.logical_and(s + k < sp, s >= 1))
+        def _():
+            tok_push(s + k, 2 * k + 1, s - 1).wait_send()
+
+    loads[0].wait()
+    token_stage(0, False)
+    for load in loads[1:5]:
+        load.wait()
+    sent = []
+
+    def launch(copy):
+        copy.start()
+        sent.append(copy)
+
+    for number, target in ((0, xn), (1, yn), (2, mate)):
+        launch(wide_push(d, number, target))
+        launch(gate_push(d, number, target))
+    loads[5].wait()
+
+    def await_wide(index):
+        wide_push(index, 0, mate).wait_recv()
+        gate_push(index, 0, mate).wait_recv()
+
+    await_wide(relay_from)
+    launch(wide_push(relay_from, 3, relay_to))
+    launch(gate_push(relay_from, 3, relay_to))
+    launch(wide_push(relay_from, 4, mate))
+    launch(gate_push(relay_from, 4, mate))
+    for part in range(PARTS):
+        for number, target in ((0, xn), (1, yn), (2, mate)):
+            launch(outw_push(d, part, number, target))
+    await_wide(relay_to)
+    launch(wide_push(relay_to, 5, mate))
+    launch(gate_push(relay_to, 5, mate))
+    token_stage(1, True)
+    await_wide(diag)
+    launch(wide_push(diag, 6, mate))
+    launch(gate_push(diag, 6, mate))
+    for k in range(2, sp):
+        token_stage(k, True)
+    for index in (mate, xn + hop, yn + hop, diag + hop):
+        await_wide(index)
+
+    flat = tok[...].reshape(rows, tok.shape[2])
+    projected = jnp.dot(flat, wide[...], preferred_element_type=jnp.float32).astype(jnp.bfloat16)
+    queries = projected[:, :key_cols]
+    keys = projected[:, key_cols : 2 * key_cols]
+    values = projected[:, 2 * key_cols :]
+    slabs = wide.shape[0] // slab
+    first = jnp.concatenate(
+        [flat[:, i * slab : i * slab + gate_rows] for i in range(slabs)], axis=1
+    )
+    second = jnp.concatenate(
+        [flat[:, i * slab + gate_rows : (i + 1) * slab] for i in range(slabs)], axis=1
+    )
+    gate_first = jnp.dot(first, gates[...], preferred_element_type=jnp.float32)
+    gate_second = jnp.dot(second, gates[...], preferred_element_type=jnp.float32)
+    gate_lanes = gate_first.shape[1]
+    pre = gate_first + pltpu.roll(gate_second, gate_lanes // 2, 1)
+    pre = pltpu.roll(pre, (gate_lanes - s * local_heads) % gate_lanes, 1)
+
+    def outw_relay(part):
+        outw_push(relay_from, part, 0, mate).wait_recv()
+        launch(outw_push(relay_from, part, 3, relay_to))
+        launch(outw_push(relay_from, part, 4, mate))
+
+    for part in range(PARTS - 1):
+        outw_relay(part)
+
+    bias_parts = []
+    for role in range(4):
+        bias_parts.append(bias_ref[role : role + 1, :])
+        bias_parts.append(jnp.zeros((1, head_count - local_heads), jnp.float32))
+    bias_parts.append(jnp.zeros((1, gate_lanes - 4 * head_count), jnp.float32))
+    pre = pre + jnp.concatenate(bias_parts, axis=1)
+    log_forget = jnp.minimum(pre, 0.0) - jnp.log1p(jnp.exp(-jnp.abs(pre)))
+    lane = lax.broadcasted_iota(jnp.int32, pre.shape, 1)
+    is_forward = lane < 2 * head_count
+    forget_sum = jnp.where(
+        is_forward,
+        scan_rows(log_forget, jnp.add, 0.0, False),
+        scan_rows(log_forget, jnp.add, 0.0, True),
+    )
+    forget_sum = pltpu.roll(forget_sum, gate_lanes - head_count, 1)
+    source = pre - forget_sum
+    peak = jnp.where(
+        is_forward,
+        scan_rows(source, jnp.maximum, -jnp.inf, False),
+        scan_rows(source, jnp.maximum, -jnp.inf, True),
+    )
+    peak = jnp.maximum(peak, 0.0)
+    floor = jnp.exp(-(forget_sum + peak))
+    source_rows = jnp.transpose(source)
+
+    row_index = lax.broadcasted_iota(jnp.int32, (rows, rows), 0)
+    col_index = lax.broadcasted_iota(jnp.int32, (rows, rows), 1)
+    masks = (col_index <= row_index, col_index >= row_index)
+    key_lane = lax.broadcasted_iota(jnp.int32, queries.shape, 1) // key_width
+    value_lane = lax.broadcasted_iota(jnp.int32, values.shape, 1) // value_width
+    scale = key_width ** (-0.5)
+    combined = jnp.zeros(values.shape, jnp.float32)
+    for h in range(local_heads):
+        head_query = jnp.where(key_lane == h, queries, jnp.zeros_like(queries))
+        head_value = jnp.where(value_lane == h, values, jnp.zeros_like(values))
+        raw = (
+            lax.dot_general(
+                head_query, keys, (((1,), (1,)), ((), ())), preferred_element_type=jnp.float32
+            )
+            * scale
+        )
+        for direction in range(2):
+            at = 2 * head_count * direction + h
+            exponent = source_rows[at : at + 1, :] - peak[:, at : at + 1]
+            weights = raw * jnp.exp(jnp.where(masks[direction], exponent, -jnp.inf))
+            total = jnp.sum(weights, axis=1, keepdims=True)
+            inverse = 1.0 / jnp.maximum(jnp.abs(total), floor[:, at : at + 1])
+            part_sum = jnp.dot(
+                weights.astype(jnp.bfloat16), head_value, preferred_element_type=jnp.float32
+            )
+            combined = combined + part_sum * inverse
+    same_head = (
+        lax.broadcasted_iota(jnp.int32, (value_cols, value_cols), 0) // value_width
+        == lax.broadcasted_iota(jnp.int32, (value_cols, value_cols), 1) // value_width
+    )
+    mean_square = jnp.dot(
+        combined * combined,
+        jnp.where(same_head, 1.0 / value_width, 0.0),
+        precision=lax.Precision.HIGHEST,
+        preferred_element_type=jnp.float32,
+    )
+    gain = jnp.concatenate([gain_ref[h : h + 1, :] for h in range(local_heads)], axis=1)
+    normed = combined * lax.rsqrt(mean_square + norm_eps) * gain
+    normed_buf[...] = normed.astype(jnp.bfloat16).reshape(sp, block, value_cols)
+
+    def norm_push(offset):
+        target = (s + offset) % sp
+        return pltpu.make_async_remote_copy(
+            src_ref=normed_buf.at[target],
+            dst_ref=hidden.at[s],
+            send_sem=norm_send.at[offset - 1],
+            recv_sem=norm_recv.at[offset - 1],
+            device_id={"sp": target},
+            device_id_type=MESH,
+        )
+
+    for offset in range(1, sp):
+        launch(norm_push(offset))
+    outw_relay(PARTS - 1)
+    hidden[s] = normed_buf[s]
+
+    for part in range(PARTS):
+        outw_push(relay_to, part, 0, mate).wait_recv()
+        launch(outw_push(relay_to, part, 5, mate))
+    for offset in range(1, sp):
+        pltpu.make_async_remote_copy(
+            src_ref=normed_buf.at[s],
+            dst_ref=hidden.at[(s + sp - offset) % sp],
+            send_sem=norm_send.at[offset - 1],
+            recv_sem=norm_recv.at[offset - 1],
+            device_id={"sp": s},
+            device_id_type=MESH,
+        ).wait_recv()
+
+    width = outw.shape[2]
+
+    def project(index):
+        total = jnp.zeros((block, width), jnp.float32)
+        for i in range(sp):
+            total = total + jnp.dot(
+                hidden[i],
+                outw[index, pl.ds(i * value_cols, value_cols), :],
+                preferred_element_type=jnp.float32,
+            )
+        out_ref[:, pl.ds(pl.multiple_of(index * width, width), width)] = total.astype(
+            out_ref.dtype
+        )
+
+    for index in (d, xn, yn):
+        project(index)
+    for part in range(PARTS):
+        outw_push(diag, part, 0, mate).wait_recv()
+        launch(outw_push(diag, part, 6, mate))
+    for index in (mate, xn + hop, yn + hop):
+        for part in range(PARTS):
+            outw_push(index, part, 0, mate).wait_recv()
+        project(index)
+    project(diag)
+    for part in range(PARTS):
+        outw_push(diag + hop, part, 0, mate).wait_recv()
+    project(diag + hop)
+    for copy in sent:
+        copy.wait_send()
+    for k in range(sp):
+        token_drain(k)
+
+
+def fused_local(
+    sp, dp, tokens, query_weight, key_weight, value_weight, gate_weight, gate_bias, norm_gain, out_weight
+):
+    block, width = tokens.shape[1], tokens.shape[2]
+    slab, roles, head_count = gate_weight.shape
+    flat_gate = gate_weight.reshape(slab, roles * head_count)
+    packed_gate = jnp.concatenate([flat_gate[: slab // 2], flat_gate[slab // 2 :]], axis=1)
+    value_cols = value_weight.shape[1] // sp
+    wide_cols = (2 * query_weight.shape[1] + value_weight.shape[1]) // sp
+    anywhere = pl.BlockSpec(memory_space=pl.ANY)
+    vmem = pl.BlockSpec(memory_space=pltpu.VMEM)
+    dma = pltpu.SemaphoreType.DMA
+    bf16 = jnp.bfloat16
+    output = pl.pallas_call(
+        functools.partial(fused_kernel, sp, head_count),
+        out_shape=jax.ShapeDtypeStruct((block, width), tokens.dtype),
+        in_specs=[anywhere] * 6 + [vmem] * 2,
+        out_specs=vmem,
+        scratch_shapes=[
+            pltpu.VMEM((sp, block, width), bf16),
+            pltpu.VMEM((dp * slab, wide_cols), bf16),
+            pltpu.VMEM((dp * packed_gate.shape[0], packed_gate.shape[1]), bf16),
+            pltpu.VMEM((dp,) + out_weight.shape, bf16),
+            pltpu.VMEM((sp, block, value_cols), bf16),
+            pltpu.VMEM((sp, block, value_cols), bf16),
+            dma((6,)),
+            dma((2 * sp,)),
+            dma((sp,)),
+            dma((7,)),
+            dma((dp,)),
+            dma((7,)),
+            dma((dp,)),
+            dma((7, PARTS)),
+            dma((dp, PARTS)),
+            dma((sp - 1,)),
+            dma((sp - 1,)),
+        ],
+        compiler_params=pltpu.CompilerParams(collective_id=0, has_side_effects=True),
+    )(
+        tokens[0],
+        query_weight,
+        key_weight,
+        value_weight,
+        packed_gate,
+        out_weight,
+        gate_bias,
+        norm_gain,
+    )
+    return output[None]
+
+
+def choose(
+    sp, dp, tokens, query_weight, key_weight, value_weight, gate_weight, gate_bias, norm_gain, out_weight
+):
+    args = (tokens, query_weight, key_weight, value_weight, gate_weight, gate_bias, norm_gain, out_weight)
+    plane_of_four_chips = dp == 2 * 2 * 2
+    aligned = (
+        tokens.shape[0] == 1
+        and query_weight.shape[1] % (128 * sp) == 0
+        and value_weight.shape[1] % (128 * sp) == 0
+        and gate_weight.shape[1] * gate_weight.shape[2] == 64
+    )
+    if plane_of_four_chips and aligned:
+        return fused_local(sp, dp, *args)
+    return local(*args)
+
+
 def solution(mesh):
     return jax.shard_map(
-        local,
+        functools.partial(choose, mesh.shape["sp"], mesh.shape["dp"]),
         mesh=mesh,
         in_specs=(
             P("dp", "sp", None),

time: 175 us -> 43.5 us (0.25)
  waiting for transfers between devices: 70 us -> 0 us
  Pallas kernels: 0 us -> 39.8 us
  matrix products: 26.6 us -> 0 us
  blocking collectives: 20.6 us -> 0 us
  starting transfers between devices: 18.8 us -> 0 us
  between operations: 13.5 us -> 0.02 us
  local copies, waits for them, and re-layouts: 15.5 us -> 2.64 us
  other arithmetic: 8.71 us -> 0.71 us
    all_gather x4 -> x0, waiting for transfers between devices: 51.6 us -> none  [the longest x3 51.6 us: local(): lax.all_gather(part, 'dp', axis=0, tiled=True)]
    pallas_call x0 -> x1, Pallas kernels: none -> 39.8 us  [fused_local(): pl.pallas_call(functools.partial(fused_kernel, sp, head_count), out_shape...]
    dot_general x53 -> x0, matrix products: 26.6 us -> none  [the longest x4 7.38 us: add_product(): jnp.dot(columns, weight_rows.reshape(row_count, -1), preferred_element_ty...]
    all_to_all x4 -> x0, starting transfers between devices: 18.7 us -> none  [the longest x1 4.87 us: local(): lax.all_to_all(gate_local, 'sp', split_axis=3, concat_axis=1, tiled=True)]
    all_to_all x4 -> x0, waiting for transfers between devices: 15.8 us -> none  [the longest x1 6.53 us: local(): lax.all_to_all(value_local, 'sp', split_axis=2, concat_axis=1, tiled=True)]
    all_gather x1 -> x0, blocking collectives: 11.6 us -> none  [local(): lax.all_gather(part, 'dp', axis=0, tiled=True)]
    all_to_all x1 -> x0, blocking collectives: 9.04 us -> none  [local(): lax.all_to_all(normed, 'sp', split_axis=1, concat_axis=2, tiled=True)]
    reduce_max x16 -> x0, other arithmetic: 2.96 us -> none  [the longest x8 1.49 us: advance(): new_stabilizer = jnp.maximum(forget_total + stabilizer, jnp.max(weights_in))]
  transfers between devices with their start and end apart: 8 -> 0, of which waited for: 6 -> 0; matrix products, arithmetic and copies ran while one was open for 27% -> 0% of each run, Pallas kernels for 0% -> 0%
where the time goes in v1:
time: 43.5 us; the launch traced here: 43.1 us
  Pallas kernels  39.8 us (91%)
  local copies, waits for them, and re-layouts  2.64 us (6%)
  other arithmetic  0.71 us (2%)
    pallas_call x1, Pallas kernels, fused_local(): pl.pallas_call(functools.partial(fused_kernel, sp, head_count), out_shape...  39.8 us
    unnamed x1, local copies, waits for them, and re-layouts  1.67 us

profile of v1, /device:TPU:0, one launch (start us, length us, event | category | flops | bytes accessed | tf_op | source)
XLA Modules:
  0.0 43.1 jit_solution(12063641764275792556)
XLA Ops:
  0.0 0.7 %fusion = (bf16[128,4,16]{0,2,1:T(8,128)(2,1)S(1)}, bf16[128,4,16]{0,2,1:T(8,128)(2,1)S(1)}) fusion(bf16[256,4,16]{0,2,1:T(8,128)(2,1)} %param.12), kind=kLoop, calls=%fused_computation.1 | loop fusion | bytes 65536 | tf_op jit(solution)/shard_map/slice | solution.py:558
  0.7 0.1 copy.12
  0.9 0.1 copy.11
  1.0 0.7 %pad_maximum_fusion.gate_ref = bf16[128,128]{1,0:T(8,128)(2,1)} fusion(bf16[128,64]{1,0:T(8,128)(2,1)S(1)} %copy.12, bf16[128,64]{1,0:T(8,128)(2,1)S(1)} %copy.11), kind=kLoop, calls=%fused_computation | loop fusion | flops 65536 | bytes 65536 | tf_op jit(solution)/shard_map/concatenate | solution.py:558
  1.7 39.8 %shard_map.82 = bf16[64,2048]{1,0:T(8,128)(2,1)} custom-call(bf16[64,2048]{1,0:T(8,128)(2,1)} %bitcast.5, bf16[256,512]{1,0:T(8,128)(2,1)} %query_ref.1, bf16[256,512]{1,0:T(8,128)(2,1)} %key_ref.1, bf16[256,1024]{1,0:T(8,128)(2,1)} %value_ref.1, bf16[128,128]{1,0:T(8,128)(2,1)} %pad_maximum_fusion.gate_ref, bf16[1024,256]{1,0:T(8,128)(2,1)} %out_weight_ref.1, ...), custom_call_target="tpu_custom_call" | custom-call | tf_op jit(solution)/shard_map/pallas_call | solution.py:565
  41.5 1.7 %copy.14 = bf16[1,64,2048]{2,1,0:T(8,128)(2,1)} copy(bf16[1,64,2048]{2,1,0:T(8,128)(2,1)} %bitcast.4) | data formatting | bytes 524288

commit v2 on v1

--- a/solution.py
+++ b/solution.py
@@ -177,7 +177,7 @@
 
 
 MESH = pl.DeviceIdType.MESH
-PARTS = 2
+PARTS = 4
 
 
 def scan_rows(values, combine, identity, backward):
@@ -214,9 +214,12 @@
     outw,
     normed_buf,
     hidden,
+    qkv,
+    gate_pre,
     local_sem,
     tok_send,
     tok_recv,
+    half_recv,
     wide_send,
     wide_recv,
     gate_send,
@@ -242,7 +245,7 @@
     slab = query_ref.shape[0]
     key_cols = query_ref.shape[1] // sp
     value_cols = value_ref.shape[1] // sp
-    gate_rows = gate_ref.shape[0]
+    roles_heads = gate_ref.shape[0]
     block = tokens_ref.shape[0]
     inner = out_weight_ref.shape[0]
     piece = inner // PARTS
@@ -255,7 +258,7 @@
         return wide.at[pl.ds(pl.multiple_of(index * slab, slab), slab), :]
 
     def gate_slot(index):
-        return gates.at[pl.ds(pl.multiple_of(index * gate_rows, gate_rows), gate_rows), :]
+        return gates.at[:, pl.ds(pl.multiple_of(index * slab, slab), slab)]
 
     def outw_slot(index, part):
         return outw.at[index, pl.ds(part * piece, piece), :]
@@ -323,39 +326,35 @@
         )
     pl.semaphore_wait(barrier, 3 + sp - 1)
 
+    right = (s + 1) % sp
+    left = (s + sp - 1) % sp
+    half = block // 2
+
+    def tok_half(origin, number, part, target):
+        ref = tok.at[origin, pl.ds(part * half, half), :]
+        return push(ref, tok_send.at[number], half_recv.at[part], "sp", target)
+
     def token_stage(k, wait):
-        right_origin = s - k
-        left_origin = s + k
-        has_left = right_origin >= 0
-        has_right = left_origin < sp
-        if wait:
-
-            @pl.when(has_left)
-            def _():
-                tok_push(right_origin, 0, s).wait_recv()
-
-        @pl.when(jnp.logical_and(has_left, s + 1 < sp))
-        def _():
-            tok_push(right_origin, 2 * k, s + 1).start()
-
-        if wait:
-
-            @pl.when(has_right)
-            def _():
-                tok_push(left_origin, 0, s).wait_recv()
-
-        @pl.when(jnp.logical_and(has_right, s >= 1))
-        def _():
-            tok_push(left_origin, 2 * k + 1, s - 1).start()
+        if k == 0:
+            tok_push(s, 0, right).start()
+            tok_push(s, 1, left).start()
+        if k == 1:
+            tok_push(left, 0, s).wait_recv()
+            tok_half(left, 2, 0, right).start()
+            tok_push(right, 0, s).wait_recv()
+            tok_half(right, 3, 1, left).start()
+        if k == 2:
+            far = (s + 2) % sp
+            tok_half(far, 2, 0, s).wait_recv()
+            tok_half(far, 3, 1, s).wait_recv()
 
     def token_drain(k):
-        @pl.when(jnp.logical_and(s - k >= 0, s + 1 < sp))
-        def _():
-            tok_push(s - k, 2 * k, s + 1).wait_send()
-
-        @pl.when(jnp.logical_and(s + k < sp, s >= 1))
-        def _():
-            tok_push(s + k, 2 * k + 1, s - 1).wait_send()
+        if k == 0:
+            tok_push(s, 0, right).wait_send()
+            tok_push(s, 1, left).wait_send()
+        if k == 1:
+            tok_half(left, 2, 0, right).wait_send()
+            tok_half(right, 3, 1, left).wait_send()
 
     loads[0].wait()
     token_stage(0, False)
@@ -367,14 +366,20 @@
         copy.start()
         sent.append(copy)
 
-    for number, target in ((0, xn), (1, yn), (2, mate)):
+    for number, target in ((0, relay_from), (1, relay_to), (2, mate)):
         launch(wide_push(d, number, target))
         launch(gate_push(d, number, target))
     loads[5].wait()
+    for part in range(PARTS):
+        launch(outw_push(d, part, 0, relay_from))
+        launch(outw_push(d, part, 2, mate))
 
     def await_wide(index):
         wide_push(index, 0, mate).wait_recv()
         gate_push(index, 0, mate).wait_recv()
+
+    def await_outw(index, part):
+        outw_push(index, part, 0, mate).wait_recv()
 
     await_wide(relay_from)
     launch(wide_push(relay_from, 3, relay_to))
@@ -382,8 +387,7 @@
     launch(wide_push(relay_from, 4, mate))
     launch(gate_push(relay_from, 4, mate))
     for part in range(PARTS):
-        for number, target in ((0, xn), (1, yn), (2, mate)):
-            launch(outw_push(d, part, number, target))
+        launch(outw_push(d, part, 1, relay_to))
     await_wide(relay_to)
     launch(wide_push(relay_to, 5, mate))
     launch(gate_push(relay_to, 5, mate))
@@ -391,36 +395,35 @@
     await_wide(diag)
     launch(wide_push(diag, 6, mate))
     launch(gate_push(diag, 6, mate))
-    for k in range(2, sp):
-        token_stage(k, True)
     for index in (mate, xn + hop, yn + hop, diag + hop):
         await_wide(index)
 
-    flat = tok[...].reshape(rows, tok.shape[2])
-    projected = jnp.dot(flat, wide[...], preferred_element_type=jnp.float32).astype(jnp.bfloat16)
+    gate_lanes = 2 * roles_heads
+
+    def project_block(index):
+        flat = tok[index]
+        qkv[index] = jnp.dot(flat, wide[...], preferred_element_type=jnp.float32).astype(
+            jnp.bfloat16
+        )
+        gate_pre[index, :, :roles_heads] = lax.dot_general(
+            flat, gates[...], (((1,), (1,)), ((), ())), preferred_element_type=jnp.float32
+        )
+
+    gate_pre[...] = jnp.zeros_like(gate_pre)
+    for index in (s, left, right):
+        project_block(index)
+    for part in range(PARTS):
+        await_outw(relay_from, part)
+        launch(outw_push(relay_from, part, 3, relay_to))
+        launch(outw_push(relay_from, part, 4, mate))
+    token_stage(2, True)
+    project_block((s + 2) % sp)
+    projected = qkv[...].reshape(rows, qkv.shape[2])
     queries = projected[:, :key_cols]
     keys = projected[:, key_cols : 2 * key_cols]
     values = projected[:, 2 * key_cols :]
-    slabs = wide.shape[0] // slab
-    first = jnp.concatenate(
-        [flat[:, i * slab : i * slab + gate_rows] for i in range(slabs)], axis=1
-    )
-    second = jnp.concatenate(
-        [flat[:, i * slab + gate_rows : (i + 1) * slab] for i in range(slabs)], axis=1
-    )
-    gate_first = jnp.dot(first, gates[...], preferred_element_type=jnp.float32)
-    gate_second = jnp.dot(second, gates[...], preferred_element_type=jnp.float32)
-    gate_lanes = gate_first.shape[1]
-    pre = gate_first + pltpu.roll(gate_second, gate_lanes // 2, 1)
+    pre = gate_pre[...].reshape(rows, gate_lanes)
     pre = pltpu.roll(pre, (gate_lanes - s * local_heads) % gate_lanes, 1)
-
-    def outw_relay(part):
-        outw_push(relay_from, part, 0, mate).wait_recv()
-        launch(outw_push(relay_from, part, 3, relay_to))
-        launch(outw_push(relay_from, part, 4, mate))
-
-    for part in range(PARTS - 1):
-        outw_relay(part)
 
     bias_parts = []
     for role in range(4):
@@ -457,18 +460,15 @@
     for h in range(local_heads):
         head_query = jnp.where(key_lane == h, queries, jnp.zeros_like(queries))
         head_value = jnp.where(value_lane == h, values, jnp.zeros_like(values))
-        raw = (
-            lax.dot_general(
-                head_query, keys, (((1,), (1,)), ((), ())), preferred_element_type=jnp.float32
-            )
-            * scale
+        raw = lax.dot_general(
+            head_query, keys, (((1,), (1,)), ((), ())), preferred_element_type=jnp.float32
         )
         for direction in range(2):
             at = 2 * head_count * direction + h
             exponent = source_rows[at : at + 1, :] - peak[:, at : at + 1]
             weights = raw * jnp.exp(jnp.where(masks[direction], exponent, -jnp.inf))
-            total = jnp.sum(weights, axis=1, keepdims=True)
-            inverse = 1.0 / jnp.maximum(jnp.abs(total), floor[:, at : at + 1])
+            total = jnp.sum(weights, axis=1, keepdims=True) * scale
+            inverse = scale / jnp.maximum(jnp.abs(total), floor[:, at : at + 1])
             part_sum = jnp.dot(
                 weights.astype(jnp.bfloat16), head_value, preferred_element_type=jnp.float32
             )
@@ -477,12 +477,14 @@
         lax.broadcasted_iota(jnp.int32, (value_cols, value_cols), 0) // value_width
         == lax.broadcasted_iota(jnp.int32, (value_cols, value_cols), 1) // value_width
     )
-    mean_square = jnp.dot(
-        combined * combined,
-        jnp.where(same_head, 1.0 / value_width, 0.0),
-        precision=lax.Precision.HIGHEST,
-        preferred_element_type=jnp.float32,
-    )
+    ones = jnp.where(same_head, 1.0, 0.0).astype(jnp.bfloat16)
+    square = combined * combined
+    square_high = square.astype(jnp.bfloat16)
+    square_low = (square - square_high.astype(jnp.float32)).astype(jnp.bfloat16)
+    mean_square = (
+        jnp.dot(square_high, ones, preferred_element_type=jnp.float32)
+        + jnp.dot(square_low, ones, preferred_element_type=jnp.float32)
+    ) * (1.0 / value_width)
     gain = jnp.concatenate([gain_ref[h : h + 1, :] for h in range(local_heads)], axis=1)
     normed = combined * lax.rsqrt(mean_square + norm_eps) * gain
     normed_buf[...] = normed.astype(jnp.bfloat16).reshape(sp, block, value_cols)
@@ -500,11 +502,10 @@
 
     for offset in range(1, sp):
         launch(norm_push(offset))
-    outw_relay(PARTS - 1)
     hidden[s] = normed_buf[s]
 
     for part in range(PARTS):
-        outw_push(relay_to, part, 0, mate).wait_recv()
+        await_outw(relay_to, part)
         launch(outw_push(relay_to, part, 5, mate))
     for offset in range(1, sp):
         pltpu.make_async_remote_copy(
@@ -554,8 +555,7 @@
 ):
     block, width = tokens.shape[1], tokens.shape[2]
     slab, roles, head_count = gate_weight.shape
-    flat_gate = gate_weight.reshape(slab, roles * head_count)
-    packed_gate = jnp.concatenate([flat_gate[: slab // 2], flat_gate[slab // 2 :]], axis=1)
+    gate_rows = jnp.transpose(gate_weight, (1, 2, 0)).reshape(roles * head_count, slab)
     value_cols = value_weight.shape[1] // sp
     wide_cols = (2 * query_weight.shape[1] + value_weight.shape[1]) // sp
     anywhere = pl.BlockSpec(memory_space=pl.ANY)
@@ -570,13 +570,16 @@
         scratch_shapes=[
             pltpu.VMEM((sp, block, width), bf16),
             pltpu.VMEM((dp * slab, wide_cols), bf16),
-            pltpu.VMEM((dp * packed_gate.shape[0], packed_gate.shape[1]), bf16),
+            pltpu.VMEM((roles * head_count, dp * slab), bf16),
             pltpu.VMEM((dp,) + out_weight.shape, bf16),
             pltpu.VMEM((sp, block, value_cols), bf16),
             pltpu.VMEM((sp, block, value_cols), bf16),
+            pltpu.VMEM((sp, block, wide_cols), bf16),
+            pltpu.VMEM((sp, block, 2 * roles * head_count), jnp.float32),
             dma((6,)),
             dma((2 * sp,)),
             dma((sp,)),
+            dma((2,)),
             dma((7,)),
             dma((dp,)),
             dma((7,)),
@@ -592,7 +595,7 @@
         query_weight,
         key_weight,
         value_weight,
-        packed_gate,
+        gate_rows,
         out_weight,
         gate_bias,
         norm_gain,
@@ -611,7 +614,7 @@
         and value_weight.shape[1] % (128 * sp) == 0
         and gate_weight.shape[1] * gate_weight.shape[2] == 64
     )
-    if plane_of_four_chips and aligned:
+    if plane_of_four_chips and sp == 2 + 2 and aligned:
         return fused_local(sp, dp, *args)
     return local(*args)
 

time: 43.5 us -> 38.9 us (0.89)
  Pallas kernels: 39.8 us -> 37.1 us
  local copies, waits for them, and re-layouts: 2.64 us -> 1.67 us
  other arithmetic: 0.71 us -> 0 us
    pallas_call x1, Pallas kernels: 39.8 us -> 37.1 us  [fused_local(): pl.pallas_call(functools.partial(fused_kernel, sp, head_count), out_shape...]
    slice x3 -> x0, local copies, waits for them, and re-layouts: 0.97 us -> none  [the longest x2 0.86 us: fused_local(): flat_gate[:slab // 2]]
    concatenate x1 -> x0, other arithmetic: 0.71 us -> none  [fused_local(): jnp.concatenate([flat_gate[:slab // 2], flat_gate[slab // 2:]], axis=1)]
where the time goes in v2:
time: 38.9 us; the launch traced here: 38.8 us
  Pallas kernels  37.1 us (95%)
  local copies, waits for them, and re-layouts  1.67 us (4%)
    pallas_call x1, Pallas kernels, fused_local(): pl.pallas_call(functools.partial(fused_kernel, sp, head_count), out_shape...  37.1 us
    unnamed x1, local copies, waits for them, and re-layouts  1.67 us

profile of v2, /device:TPU:0, one launch (start us, length us, event | category | flops | bytes accessed | tf_op | source)
XLA Modules:
  0.0 38.8 jit_solution(17780327329519509688)
XLA Ops:
  0.0 37.1 %shard_map.82 = bf16[64,2048]{1,0:T(8,128)(2,1)} custom-call(bf16[64,2048]{1,0:T(8,128)(2,1)} %bitcast.6, bf16[256,512]{1,0:T(8,128)(2,1)} %query_ref.1, bf16[256,512]{1,0:T(8,128)(2,1)} %key_ref.1, bf16[256,1024]{1,0:T(8,128)(2,1)} %value_ref.1, bf16[64,256]{1,0:T(8,128)(2,1)} %bitcast.7, bf16[1024,256]{1,0:T(8,128)(2,1)} %out_weight_ref.1, ...), custom_call_target="tpu_custom_call" | custom-call | tf_op jit(solution)/shard_map/pallas_call | solution.py:565
  37.1 1.7 %copy.10 = bf16[1,64,2048]{2,1,0:T(8,128)(2,1)} copy(bf16[1,64,2048]{2,1,0:T(8,128)(2,1)} %bitcast.5) | data formatting | bytes 524288

commit v3 on v2

--- a/solution.py
+++ b/solution.py
@@ -211,10 +211,12 @@
     tok,
     wide,
     gates,
+    gate_all,
     outw,
     normed_buf,
     hidden,
     qkv,
+    total_out,
     gate_pre,
     local_sem,
     tok_send,
@@ -311,7 +313,7 @@
             wide.at[own_rows, pl.ds(2 * key_cols, value_cols)],
             local_sem.at[3],
         ),
-        pltpu.make_async_copy(gate_ref, gate_slot(d), local_sem.at[4]),
+        pltpu.make_async_copy(gate_ref, gate_all, local_sem.at[4]),
         pltpu.make_async_copy(out_weight_ref, outw.at[d], local_sem.at[5]),
     ]
     for load in loads:
@@ -366,8 +368,18 @@
         copy.start()
         sent.append(copy)
 
+    own_gates = roles_heads // sp
+    picked = lax.broadcasted_iota(jnp.int32, (own_gates, roles_heads), 0)
+    wanted = picked // local_heads * head_count + s * local_heads + picked % local_heads
+    chooser = jnp.where(
+        lax.broadcasted_iota(jnp.int32, (own_gates, roles_heads), 1) == wanted, 1.0, 0.0
+    ).astype(jnp.bfloat16)
+    gates[:, pl.ds(pl.multiple_of(d * slab, slab), slab)] = jnp.dot(
+        chooser, gate_all[...], preferred_element_type=jnp.float32
+    ).astype(jnp.bfloat16)
     for number, target in ((0, relay_from), (1, relay_to), (2, mate)):
         launch(wide_push(d, number, target))
+    for number, target in ((0, relay_from), (1, relay_to), (2, mate)):
         launch(gate_push(d, number, target))
     loads[5].wait()
     for part in range(PARTS):
@@ -395,6 +407,11 @@
     await_wide(diag)
     launch(wide_push(diag, 6, mate))
     launch(gate_push(diag, 6, mate))
+    gate_pre[...] = jnp.zeros_like(gate_pre)
+    for part in range(PARTS - 2):
+        await_outw(relay_from, part)
+        launch(outw_push(relay_from, part, 3, relay_to))
+        launch(outw_push(relay_from, part, 4, mate))
     for index in (mate, xn + hop, yn + hop, diag + hop):
         await_wide(index)
 
@@ -405,17 +422,21 @@
         qkv[index] = jnp.dot(flat, wide[...], preferred_element_type=jnp.float32).astype(
             jnp.bfloat16
         )
-        gate_pre[index, :, :roles_heads] = lax.dot_general(
+        gate_pre[index, :, :own_gates] = lax.dot_general(
             flat, gates[...], (((1,), (1,)), ((), ())), preferred_element_type=jnp.float32
         )
 
-    gate_pre[...] = jnp.zeros_like(gate_pre)
-    for index in (s, left, right):
-        project_block(index)
-    for part in range(PARTS):
+    def outw_relay(part):
         await_outw(relay_from, part)
         launch(outw_push(relay_from, part, 3, relay_to))
         launch(outw_push(relay_from, part, 4, mate))
+
+    project_block(s)
+    for part in range(PARTS - 2, PARTS - 1):
+        outw_relay(part)
+    project_block(left)
+    outw_relay(PARTS - 1)
+    project_block(right)
     token_stage(2, True)
     project_block((s + 2) % sp)
     projected = qkv[...].reshape(rows, qkv.shape[2])
@@ -423,23 +444,21 @@
     keys = projected[:, key_cols : 2 * key_cols]
     values = projected[:, 2 * key_cols :]
     pre = gate_pre[...].reshape(rows, gate_lanes)
-    pre = pltpu.roll(pre, (gate_lanes - s * local_heads) % gate_lanes, 1)
 
     bias_parts = []
     for role in range(4):
         bias_parts.append(bias_ref[role : role + 1, :])
-        bias_parts.append(jnp.zeros((1, head_count - local_heads), jnp.float32))
-    bias_parts.append(jnp.zeros((1, gate_lanes - 4 * head_count), jnp.float32))
+    bias_parts.append(jnp.zeros((1, gate_lanes - 4 * local_heads), jnp.float32))
     pre = pre + jnp.concatenate(bias_parts, axis=1)
     log_forget = jnp.minimum(pre, 0.0) - jnp.log1p(jnp.exp(-jnp.abs(pre)))
     lane = lax.broadcasted_iota(jnp.int32, pre.shape, 1)
-    is_forward = lane < 2 * head_count
+    is_forward = lane < 2 * local_heads
     forget_sum = jnp.where(
         is_forward,
         scan_rows(log_forget, jnp.add, 0.0, False),
         scan_rows(log_forget, jnp.add, 0.0, True),
     )
-    forget_sum = pltpu.roll(forget_sum, gate_lanes - head_count, 1)
+    forget_sum = pltpu.roll(forget_sum, gate_lanes - local_heads, 1)
     source = pre - forget_sum
     peak = jnp.where(
         is_forward,
@@ -464,7 +483,7 @@
             head_query, keys, (((1,), (1,)), ((), ())), preferred_element_type=jnp.float32
         )
         for direction in range(2):
-            at = 2 * head_count * direction + h
+            at = 2 * local_heads * direction + h
             exponent = source_rows[at : at + 1, :] - peak[:, at : at + 1]
             weights = raw * jnp.exp(jnp.where(masks[direction], exponent, -jnp.inf))
             total = jnp.sum(weights, axis=1, keepdims=True) * scale
@@ -504,9 +523,35 @@
         launch(norm_push(offset))
     hidden[s] = normed_buf[s]
 
+    width = outw.shape[2]
+
+    def own_part(index):
+        column = pl.ds(pl.multiple_of(index * width, width), width)
+        own = pl.ds(pl.multiple_of(s * value_cols, value_cols), value_cols)
+        total_out[:, column] = jnp.dot(
+            hidden[s], outw[index, own, :], preferred_element_type=jnp.float32
+        )
+
+    def project(index):
+        column = pl.ds(pl.multiple_of(index * width, width), width)
+        total = total_out[:, column]
+        for offset in range(1, sp):
+            i = (s + offset) % sp
+            taken = pl.ds(pl.multiple_of(i * value_cols, value_cols), value_cols)
+            total = total + jnp.dot(
+                hidden[i], outw[index, taken, :], preferred_element_type=jnp.float32
+            )
+        out_ref[:, column] = total.astype(out_ref.dtype)
+
+    own_part(d)
+    own_part(relay_from)
     for part in range(PARTS):
         await_outw(relay_to, part)
         launch(outw_push(relay_to, part, 5, mate))
+    own_part(relay_to)
+    for part in range(PARTS):
+        await_outw(mate, part)
+    own_part(mate)
     for offset in range(1, sp):
         pltpu.make_async_remote_copy(
             src_ref=normed_buf.at[s],
@@ -516,33 +561,22 @@
             device_id={"sp": s},
             device_id_type=MESH,
         ).wait_recv()
-
-    width = outw.shape[2]
-
-    def project(index):
-        total = jnp.zeros((block, width), jnp.float32)
-        for i in range(sp):
-            total = total + jnp.dot(
-                hidden[i],
-                outw[index, pl.ds(i * value_cols, value_cols), :],
-                preferred_element_type=jnp.float32,
-            )
-        out_ref[:, pl.ds(pl.multiple_of(index * width, width), width)] = total.astype(
-            out_ref.dtype
-        )
-
-    for index in (d, xn, yn):
+    for part in range(PARTS):
+        await_outw(diag, part)
+        launch(outw_push(diag, part, 6, mate))
+        if part < PARTS - 1:
+            project((d, relay_from, relay_to)[part % 3])
+    project(mate)
+    for index in (xn + hop, yn + hop):
+        for part in range(PARTS):
+            await_outw(index, part)
+        own_part(index)
         project(index)
-    for part in range(PARTS):
-        outw_push(diag, part, 0, mate).wait_recv()
-        launch(outw_push(diag, part, 6, mate))
-    for index in (mate, xn + hop, yn + hop):
-        for part in range(PARTS):
-            outw_push(index, part, 0, mate).wait_recv()
-        project(index)
+    own_part(diag)
     project(diag)
     for part in range(PARTS):
-        outw_push(diag + hop, part, 0, mate).wait_recv()
+        await_outw(diag + hop, part)
+    own_part(diag + hop)
     project(diag + hop)
     for copy in sent:
         copy.wait_send()
@@ -558,7 +592,7 @@
     gate_rows = jnp.transpose(gate_weight, (1, 2, 0)).reshape(roles * head_count, slab)
     value_cols = value_weight.shape[1] // sp
     wide_cols = (2 * query_weight.shape[1] + value_weight.shape[1]) // sp
-    anywhere = pl.BlockSpec(memory_space=pl.ANY)
+    anywhere = pl.BlockSpec(memory_space=pltpu.HBM)
     vmem = pl.BlockSpec(memory_space=pltpu.VMEM)
     dma = pltpu.SemaphoreType.DMA
     bf16 = jnp.bfloat16
@@ -570,11 +604,13 @@
         scratch_shapes=[
             pltpu.VMEM((sp, block, width), bf16),
             pltpu.VMEM((dp * slab, wide_cols), bf16),
-            pltpu.VMEM((roles * head_count, dp * slab), bf16),
+            pltpu.VMEM((roles * head_count // sp, dp * slab), bf16),
+            pltpu.VMEM((roles * head_count, slab), bf16),
             pltpu.VMEM((dp,) + out_weight.shape, bf16),
             pltpu.VMEM((sp, block, value_cols), bf16),
             pltpu.VMEM((sp, block, value_cols), bf16),
             pltpu.VMEM((sp, block, wide_cols), bf16),
+            pltpu.VMEM((block, width), jnp.float32),
             pltpu.VMEM((sp, block, 2 * roles * head_count), jnp.float32),
             dma((6,)),
             dma((2 * sp,)),

time: 38.9 us -> 38.3 us (0.985)
  Pallas kernels: 37.1 us -> 36.4 us
    pallas_call x1, Pallas kernels: 37.1 us -> 36.4 us  [fused_local(): pl.pallas_call(functools.partial(fused_kernel, sp, head_count), out_shape...]
where the time goes in v3:
time: 38.3 us; the launch traced here: 38.1 us
  Pallas kernels  36.4 us (95%)
  local copies, waits for them, and re-layouts  1.67 us (4%)
    pallas_call x1, Pallas kernels, fused_local(): pl.pallas_call(functools.partial(fused_kernel, sp, head_count), out_shape...  36.4 us
    unnamed x1, local copies, waits for them, and re-layouts  1.67 us

profile of v3, /device:TPU:0, one launch (start us, length us, event | category | flops | bytes accessed | tf_op | source)
XLA Modules:
  0.0 38.1 jit_solution(10405260535343644662)
XLA Ops:
  0.0 36.4 %shard_map.82 = bf16[64,2048]{1,0:T(8,128)(2,1)} custom-call(bf16[64,2048]{1,0:T(8,128)(2,1)} %bitcast.6, bf16[256,512]{1,0:T(8,128)(2,1)} %query_ref.1, bf16[256,512]{1,0:T(8,128)(2,1)} %key_ref.1, bf16[256,1024]{1,0:T(8,128)(2,1)} %value_ref.1, bf16[64,256]{1,0:T(8,128)(2,1)} %bitcast.7, bf16[1024,256]{1,0:T(8,128)(2,1)} %out_weight_ref.1, ...), custom_call_target="tpu_custom_call" | custom-call | tf_op jit(solution)/shard_map/pallas_call | solution.py:599
  36.4 1.7 %copy.10 = bf16[1,64,2048]{2,1,0:T(8,128)(2,1)} copy(bf16[1,64,2048]{2,1,0:T(8,128)(2,1)} %bitcast.5) | data formatting | bytes 524288
